TPU v7x, 32 devices: a whole 2x2x4 slice. The times are simulated.
32 devices in a mesh: row: 16 (over z, y, x), col: 2 (over core).
Axes of the slice: x: 2, y: 2, z: 4, core: 2. Of those that a mesh axis runs over, the one named last changes fastest.
Arguments:
- tokens: bfloat16 [2, 3072, 2048], P('col', 'row'), may hold values from -6 to 6
- proj_in: bfloat16 [2048, 512], P('col'), may hold values from -0.125 to 0.125
- proj_out: bfloat16 [512, 2048], P(None, 'row'), may hold values from -0.25 to 0.25
Outputs:
- output: bfloat16 [2, 3072, 2048], P('col', 'row')
All inputs are finite; a program needn't handle non-finite values.
Results may differ from a plain program's by a relative error of at most 0.0083.
Values may be sent and summed in bfloat16 or wider, within the bound.
No kernel may reach another device: no remote copies, remote signals or barrier semaphores. Data moves between devices by JAX's collectives and lax.ppermute only.
A program may use at most 64 MiB of HBM per device.

v0:
```python
import math

import jax
import jax.numpy as jnp
from jax import lax
from jax.sharding import PartitionSpec as P

GRP = 128


highest = lax.Precision.HIGHEST
span_inner = 128


def circle(height, breadth, period):
    product = lax.iota(jnp.int32, height)[:, None] * lax.iota(jnp.int32, breadth)[None, :] % period
    angle = product.astype(jnp.float32) * (2.0 * math.pi / period)
    return (jnp.cos(angle), jnp.sin(angle))


def positions(piece):
    real_in = piece[0, 0]
    imag_in = piece[1, 0]
    count, length = real_in.shape
    outer = length // span_inner
    real_in = real_in.reshape(count, outer, span_inner)
    imag_in = imag_in.reshape(count, outer, span_inner)
    cos_one, sin_one = circle(outer, outer, outer)
    first_re = jnp.einsum("ab,kbq->kaq", cos_one, real_in, precision=highest) - jnp.einsum(
        "ab,kbq->kaq", sin_one, imag_in, precision=highest
    )
    first_im = jnp.einsum("ab,kbq->kaq", sin_one, real_in, precision=highest) + jnp.einsum(
        "ab,kbq->kaq", cos_one, imag_in, precision=highest
    )
    twist_c, twist_s = circle(outer, span_inner, length)
    turned_re = first_re * twist_c - first_im * twist_s
    turned_im = first_re * twist_s + first_im * twist_c
    cos_two, sin_two = circle(span_inner, span_inner, span_inner)
    factor = 1.0 / math.sqrt(GRP * length)
    real_out = jnp.einsum("kaq,qb->kba", turned_re, cos_two, precision=highest) - jnp.einsum(
        "kaq,qb->kba", turned_im, sin_two, precision=highest
    )
    real_out = real_out.reshape(count, length) * factor
    return real_out[:, None, :]


def shards(tokens, proj_in, proj_out):
    seq_rows = tokens[0]
    local_len = seq_rows.shape[0]
    features = proj_in.shape[1]
    groups = features // GRP
    mapped = jnp.dot(
        seq_rows,
        lax.all_gather(proj_in, "col", axis=0, tiled=True),
        preferred_element_type=jnp.float32,
    ).astype(jnp.bfloat16)
    values = mapped.astype(jnp.float32).reshape(local_len, groups, GRP)
    cos_c, sin_c = circle(GRP, GRP, GRP)
    real_part = jnp.einsum("pgc,cs->gsp", values, cos_c, precision=highest)
    imag_part = jnp.einsum("pgc,cs->gsp", values, sin_c, precision=highest)
    ways = lax.axis_size("row")
    slots = groups * cos_c.shape[1]
    per_dev = slots // ways
    stacked = jnp.stack(
        [real_part.reshape(ways, per_dev, local_len), imag_part.reshape(ways, per_dev, local_len)],
        0,
    )
    spectra = positions(lax.all_to_all(stacked, "row", split_axis=1, concat_axis=3, tiled=True))
    outgoing = spectra.astype(jnp.bfloat16)
    back = lax.all_to_all(outgoing, "row", split_axis=2, concat_axis=0, tiled=True)
    mixed = back.reshape(features, local_len)
    result = lax.dot_general(
        mixed,
        lax.all_gather(proj_out, "row", axis=1, tiled=True),
        (((0,), (0,)), ((), ())),
        preferred_element_type=jnp.float32,
    )
    return result.astype(jnp.bfloat16)[None]


def solution(mesh):
    in_specs = (P("col", "row", None), P("col", None), P(None, "row"))
    out_specs = P("col", "row", None)
    return jax.shard_map(shards, mesh=mesh, in_specs=in_specs, out_specs=out_specs, check_vma=False)
```

profile of v0, /device:TPU:0, one launch (start us, length us, event | category | flops | bytes accessed | tf_op | source)
XLA Modules:
  0.0 115.2 jit_solution(4672272364211628046)
XLA Ops:
  6.5 0.7 all-gather.3.cloned.1.call-update
  7.3 0.7 all-gather.5.cloned.1.call-update
  8.0 14.2 %all-gather.3.cloned.1.call-done = bf16[2048,512]{1,0:T(8,128)(2,1)} async-done(((bf16[1024,512]{1,0:T(8,128)(2,1)}), bf16[2048,512]{1,0:T(8,128)(2,1)}) %all-gather.3.cloned.1.call-update) | async-done | bytes 2097168 | tf_op jit(solution)/shard_map/all_gather | solution.py:54
  22.2 2.2 %fusion.5 = bf16[24,4,8,128]{3,2,1,0:T(8,128)(2,1)S(1)} fusion(bf16[2048,512]{1,0:T(8,128)(2,1)} %all-gather.3.cloned.1.call-done, bf16[1,192,2048]{2,1,0:T(8,128)(2,1)S(1)} %copy-done), kind=kOutput, calls=%fused_computation.12 | convolution fusion | flops 402751488 | bytes 3080192 | tf_op jit(solution)/shard_map/dot_general | solution.py:52
  24.4 0.6 convolution_bitcast_fusion.1
  24.9 0.2 copy.19
  25.2 0.6 convolution_bitcast_fusion
  25.7 0.2 copy.21
  26.0 1.1 copy.22
  27.1 6.8 %all-to-all-start = ((f32[2,16,32,192]{3,2,0,1:T(8,128)}), f32[2,16,32,192]{3,2,0,1:T(8,128)S(1)}, u32[]{:S(2)}, u32[]{:S(2)}) async-start(f32[2,16,32,192]{3,2,0,1:T(8,128)} %copy.22), calls=%async_computation | async-start | bytes 2097152 | tf_op jit(solution)/shard_map/all_to_all | solution.py:68
  34.0 24.7 %all-to-all-done = f32[2,16,32,192]{3,2,0,1:T(8,128)S(1)} async-done(((f32[2,16,32,192]{3,2,0,1:T(8,128)}), f32[2,16,32,192]{3,2,0,1:T(8,128)S(1)}, u32[]{:S(2)}, u32[]{:S(2)}) %all-to-all-start) | async-done | bytes 786464 | tf_op jit(solution)/shard_map/all_to_all | solution.py:68
  58.7 0.1 fusion.95
  58.8 0.3 copy.23
  59.1 0.3 reshape_squeeze.6
  59.4 0.3 copy.24
  59.7 0.3 reshape_squeeze.7
  60.0 0.5 fusion.39
  60.5 0.5 fusion.35
  61.0 0.5 fusion.2
  61.6 0.6 multiply_add_fusion
  62.2 0.7 fusion.9
  62.9 0.7 fusion.6
  63.7 0.4 copy.31
  64.1 0.4 reshape.66
  64.5 0.5 broadcast.106
  65.0 17.0 %reduce = bf16[3072,32]{1,0:T(8,128)(2,1)S(1)} reduce(bf16[3072,1,32]{2,1,0:T(2,128)(2,1)S(1)} %bitcast.68, bf16[]{:T(256)} %broadcast.106), dimensions={1}, to_apply=%bitcast.57.reduce_sub_computation | reduce | bytes 393218
  82.0 0.8 reshape.67
  82.7 19.8 %all_to_all.30 = bf16[16,2,3072]{2,1,0:T(2,128)(2,1)S(1)} all-to-all(bf16[16,2,3072]{2,1,0:T(2,128)(2,1)S(1)} %reshape.67), channel_id=1, replica_groups=mesh['row'=16,'col'=2] {'row'}, dimensions={0} | all-to-all | bytes 393216 | tf_op jit(solution)/shard_map/all_to_all | solution.py:70
  102.6 0.9 reshape.68
  103.4 1.4 %copy.29 = bf16[32,1,3072]{2,0,1:T(8,128)(2,1)S(1)} copy(bf16[32,1,3072]{0,1,2:T(2,128)(2,1)S(1)} %bitcast.69) | data formatting | bytes 393216 | tf_op jit(solution)/shard_map/all_to_all | solution.py:70
  104.8 0.3 all_to_all.26
  105.2 3.1 %fusion = bf16[1,192,2048]{2,1,0:T(8,128)(2,1)} fusion(bf16[512,192]{1,0:T(8,128)(2,1)S(1)} %bitcast.73, bf16[512,2048]{1,0:T(8,128)(2,1)} %all-gather.5.cloned.1.call-done), kind=kOutput, calls=%fused_computation.1 | convolution fusion | flops 403046400 | bytes 3080192 | tf_op jit(solution)/shard_map/dot_general | solution.py:72
  (8 shorter events, 0.3 us)
Async XLA Ops:
  6.5 15.7 %copy-start = (bf16[1,192,2048]{2,1,0:T(8,128)(2,1)S(1)}, bf16[1,192,2048]{2,1,0:T(8,128)(2,1)}, u32[]{:S(2)}) copy-start(bf16[1,192,2048]{2,1,0:T(8,128)(2,1)} %param.3) | copy-start | bytes 2359300
  6.5 15.7 %all-gather.3.cloned.1.call-start = ((), (), s32[]{:S(2)}) async-start(), calls=%async_computation.2 | async-start | bytes 3145728 | tf_op jit(solution)/shard_map/all_gather | solution.py:54
  7.3 98.0 %all-gather.5.cloned.1.call-start = ((), (), s32[]{:S(2)}) async-start(), calls=%async_computation.3 | async-start | bytes 2228224 | tf_op jit(solution)/shard_map/all_gather | solution.py:74
  27.1 31.6 %all-to-all-start = ((f32[2,16,32,192]{3,2,0,1:T(8,128)}), f32[2,16,32,192]{3,2,0,1:T(8,128)S(1)}, u32[]{:S(2)}, u32[]{:S(2)}) async-start(f32[2,16,32,192]{3,2,0,1:T(8,128)} %copy.22), calls=%async_computation | async-start | bytes 2097152 | tf_op jit(solution)/shard_map/all_to_all | solution.py:68
Sparse Core Ops, SparseCore 0:
  8.9 13.2 all-gather.2
  24.9 73.4 all-gather.4
where the time goes:
time: 115 us
  waiting for transfers between devices  40.3 us (35%)
  blocking collectives  19.8 us (17%)
  other arithmetic  17.1 us (15%)
  between operations  13.6 us (12%)
  matrix products  10 us (9%)
  local copies, waits for them, and re-layouts  7.43 us (6%)
  starting transfers between devices  6.84 us (6%)
    all_to_all x1, waiting for transfers between devices, shards(): lax.all_to_all(stacked, 'row', split_axis=1, concat_axis=3, tiled=True)  24.7 us
    all_to_all x1, blocking collectives, shards(): lax.all_to_all(outgoing, 'row', split_axis=2, concat_axis=0, tiled=True)  19.8 us
    unnamed x1, other arithmetic  17 us
    all_gather x1, waiting for transfers between devices, shards(): lax.all_gather(proj_in, 'col', axis=0, tiled=True)  14.2 us
    all_to_all x1, starting transfers between devices, shards(): lax.all_to_all(stacked, 'row', split_axis=1, concat_axis=3, tiled=True)  6.8 us
    dot_general x1, matrix products, shards(): lax.dot_general(mixed, lax.all_gather(proj_out, 'row', axis=1, tiled=True...  3.08 us
  transfers between devices with their start and end apart: 3, of which 2 were waited for; matrix products, arithmetic and copies ran while one was open for 27% of the time, Pallas kernels for 0%

commit v1 on v0

--- a/solution.py
+++ b/solution.py
@@ -2,12 +2,14 @@
 
 import jax
 import jax.numpy as jnp
+import numpy as np
 from jax import lax
+from jax.experimental import pallas as pl
+from jax.experimental.pallas import tpu as pltpu
 from jax.sharding import PartitionSpec as P
 
 GRP = 128
-
-
+LANES = 128
 highest = lax.Precision.HIGHEST
 span_inner = 128
 
@@ -44,7 +46,7 @@
     return real_out[:, None, :]
 
 
-def shards(tokens, proj_in, proj_out):
+def general_shards(tokens, proj_in, proj_out):
     seq_rows = tokens[0]
     local_len = seq_rows.shape[0]
     features = proj_in.shape[1]
@@ -78,7 +80,314 @@
     return result.astype(jnp.bfloat16)[None]
 
 
+def channel_table(quarters, pairs):
+    c = np.arange(GRP)
+    rows = []
+    for t in range(quarters):
+        j = pairs * t + np.arange(pairs)
+        angle = 2 * np.pi * (j[:, None] * c % GRP) / GRP
+        sine = np.sin(angle)
+        if t == 0:
+            sine[0] = np.cos(np.pi * c)
+        rows += [np.cos(angle), sine]
+    return np.concatenate(rows, 0)
+
+
+def channel_order(groups, quarters, pairs):
+    order = []
+    for g in range(groups):
+        for t in range(quarters):
+            j = pairs * t + np.arange(pairs)
+            mirror = (GRP - j) % GRP
+            if t == 0:
+                mirror[0] = GRP // 2
+            order += list(g * GRP + j) + list(g * GRP + mirror)
+    return np.array(order)
+
+
+def position_tables(ways, span):
+    per = span // ways
+    q = np.arange(span)
+    low = min(LANES, span)
+    even = np.zeros((ways, 16, 4 * LANES))
+    odd = np.zeros((ways, 16, 4 * LANES))
+    for owner in range(ways):
+        for m in range(per):
+            angle = 2 * np.pi * (q * (per * owner + m) % span) / span
+            row = np.zeros(4 * LANES)
+            row[:low] = np.cos(angle[:low])
+            row[LANES : LANES + low] = np.sin(angle[:low])
+            row[2 * LANES : 2 * LANES + span - low] = np.cos(angle[low:])
+            row[3 * LANES : 3 * LANES + span - low] = np.sin(angle[low:])
+            even[owner, m] = row
+            odd[owner, m if m < 8 else m + 4] = row
+    return even.reshape(-1, 4 * LANES), odd.reshape(-1, 4 * LANES)
+
+
+def twiddle_table(ways, span):
+    length = ways * span
+    factor = 1.0 / math.sqrt(GRP * length)
+    q = np.arange(2 * LANES)
+    angle = 2 * np.pi * (np.arange(ways)[:, None] * q % length) / length
+    cos, sin = np.cos(angle) * factor, np.sin(angle) * factor
+    return np.stack([cos[:, :LANES], sin[:, :LANES], cos[:, LANES:], sin[:, LANES:]], 1)
+
+
+def row_order(span):
+    chunk = []
+    chunk += [(0, m) for m in range(8)] + [(2, m) for m in range(8)]
+    for a in range(4):
+        chunk += [((0, 2, 1, 3)[a], 8 + m) for m in range(4)]
+    chunk += [(1, m) for m in range(8)] + [(3, m) for m in range(8)]
+    rows = len(chunk)
+    hot = np.zeros((span, span))
+    for b in range(4):
+        for i, (a, m) in enumerate(chunk):
+            hot[16 * m + 4 * a + b, b * rows + i] = 1
+    return hot
+
+
+def own_kernel(where, tok, w, out):
+    out[...] = jnp.dot(tok[...], w[...], preferred_element_type=jnp.float32)
+
+
+def send_kernel(where, tok, w, part, table, out, padded):
+    span, features = part.shape
+    mapped = part[...] + jnp.dot(tok[...], w[...], preferred_element_type=jnp.float32)
+    padded[pl.ds(0, span), :] = mapped.astype(jnp.bfloat16)
+    padded[pl.ds(span, 2 * LANES - span), :] = jnp.zeros((2 * LANES - span, features), jnp.bfloat16)
+    groups = features // GRP
+    quarters = out.shape[0] // groups
+    for g in range(groups):
+        turned = lax.dot_general(
+            table[...],
+            padded[:, g * GRP : (g + 1) * GRP],
+            (((1,), (1,)), ((), ())),
+            preferred_element_type=jnp.float32,
+        )
+        for t in range(quarters):
+            cos = turned[32 * t : 32 * t + 16]
+            sin = turned[32 * t + 16 : 32 * t + 32]
+            high = cos[:, LANES:] + pltpu.roll(sin[:, LANES:], LANES // 2, 1)
+            d = g * quarters + t
+            out[d, 0:16, :] = cos[:, :LANES].astype(jnp.bfloat16)
+            out[d, 16:32, :] = sin[:, :LANES].astype(jnp.bfloat16)
+            out[d, 32:48, :] = high.astype(jnp.bfloat16)
+
+
+def fft4(a, b, c, d):
+    (ar, ai), (br, bi), (cr, ci), (dr, di) = a, b, c, d
+    sr, si, tr, ti = ar + cr, ai + ci, ar - cr, ai - ci
+    ur, ui, vr, vi = br + dr, bi + di, br - dr, bi - di
+    return [(sr + ur, si + ui), (tr + vi, ti - vr), (sr - ur, si - ui), (tr - vi, ti + vr)]
+
+
+def turn(v, n):
+    re, im = v
+    n %= 16
+    if n == 0:
+        return v
+    if n == 4:
+        return (im, -re)
+    if n == 2:
+        h = math.sqrt(0.5)
+        return ((re + im) * h, (im - re) * h)
+    if n == 6:
+        h = math.sqrt(0.5)
+        return ((im - re) * h, -(re + im) * h)
+    c, s = math.cos(2 * math.pi * n / 16), math.sin(2 * math.pi * n / 16)
+    return (re * c + im * s, im * c - re * s)
+
+
+def fft16(v):
+    inner = [fft4(v[a], v[a + 4], v[a + 8], v[a + 12]) for a in range(4)]
+    out = [None] * 16
+    for f in range(4):
+        col = fft4(*[turn(inner[a][f], a * f) for a in range(4)])
+        for e in range(4):
+            out[f + 4 * e] = col[e]
+    return out
+
+
+def mix_kernel(special, x, even, odd, twist, out, turned):
+    ways = x.shape[0]
+    first = (lax.broadcasted_iota(jnp.int32, (16, LANES), 0) == 0) & (special[0] == 0)
+    for part in range(2):
+        v = []
+        for r in range(ways):
+            if part == 0:
+                re = x[r, 0:16, :].astype(jnp.float32)
+                im = -x[r, 16:32, :].astype(jnp.float32)
+            else:
+                re = x[r, 32:48, :].astype(jnp.float32)
+                im = -pltpu.roll(re, LANES // 2, 1)
+            v.append((re, im))
+        spec = fft16(v)
+        for k in range(ways):
+            pr, pi = spec[k]
+            qr, qi = spec[-k % ways]
+            qi = -qi
+            ur = jnp.where(first, (pr + qr) * 0.5, pr)
+            ui = jnp.where(first, (pi + qi) * 0.5, pi)
+            wr = jnp.where(first, (qi - pi) * 0.5, qr)
+            wi = jnp.where(first, (pr - qr) * 0.5, qi)
+            c = twist[k, 2 * part : 2 * part + 1, :]
+            s = twist[k, 2 * part + 1 : 2 * part + 2, :]
+            lo = slice(2 * part * LANES, (2 * part + 1) * LANES)
+            hi = slice((2 * part + 1) * LANES, (2 * part + 2) * LANES)
+            turned[32 * k : 32 * k + 16, lo] = (ur * c + ui * s).astype(jnp.bfloat16)
+            turned[32 * k : 32 * k + 16, hi] = (ui * c - ur * s).astype(jnp.bfloat16)
+            turned[32 * k + 16 : 32 * k + 32, lo] = (wr * c + wi * s).astype(jnp.bfloat16)
+            turned[32 * k + 16 : 32 * k + 32, hi] = (wi * c - wr * s).astype(jnp.bfloat16)
+    half = turned.shape[0] // 2
+    nt = (((1,), (1,)), ((), ()))
+    one = lax.dot_general(even[...], turned[:half, :], nt, preferred_element_type=jnp.float32)
+    two = lax.dot_general(odd[...], turned[half:, :], nt, preferred_element_type=jnp.float32)
+    for r in range(ways):
+        e, o = one[16 * r : 16 * r + 16], two[16 * r : 16 * r + 16]
+        tail = e[8:] + o[8:]
+        left, right = slice(0, LANES), slice(LANES, 2 * LANES)
+        out[r, 0:16, :] = jnp.concatenate([e[:8, left], o[:8, left]], 0).astype(jnp.bfloat16)
+        out[r, 16:32, :] = jnp.concatenate([tail[:, left], tail[:, right]], 0).astype(jnp.bfloat16)
+        out[r, 32:48, :] = jnp.concatenate([e[:8, right], o[:8, right]], 0).astype(jnp.bfloat16)
+
+
+def gather_blocks(y, groups, stage):
+    quarters = y.shape[0] // groups
+    rows = y.shape[1]
+    lane = lax.broadcasted_iota(jnp.int32, (rows, LANES), 1) // 32
+    odd, high = lane % 2 == 1, lane >= 2
+    for g in range(groups):
+        v = [y[g * quarters + t].astype(jnp.float32) for t in range(quarters)]
+        w = [None] * 4
+        for t in (0, 2):
+            w[t] = jnp.where(odd, pltpu.roll(v[t + 1], 32, 1), v[t])
+            w[t + 1] = jnp.where(odd, v[t + 1], pltpu.roll(v[t], LANES - 32, 1))
+        u = [None] * 4
+        for b in (0, 1):
+            u[b] = jnp.where(high, pltpu.roll(w[b + 2], 64, 1), w[b])
+            u[b + 2] = jnp.where(high, w[b + 2], pltpu.roll(w[b], 64, 1))
+        for b in range(4):
+            stage[b * rows : (b + 1) * rows, g * GRP : (g + 1) * GRP] = u[b].astype(jnp.bfloat16)
+
+
+def out_kernel(y, hot, w, out, stage):
+    groups = w.shape[0] // GRP
+    gather_blocks(y, groups, stage)
+    mixed = jnp.dot(hot[...], stage[...], preferred_element_type=jnp.float32).astype(jnp.bfloat16)
+    out[...] = jnp.dot(mixed, w[...], preferred_element_type=jnp.float32).astype(jnp.bfloat16)
+
+
+def vmem(count):
+    return [pl.BlockSpec(memory_space=pltpu.VMEM)] * count
+
+
+def shards(tokens, proj_in, proj_out):
+    seq_rows = tokens[0]
+    span, width = seq_rows.shape
+    depth, features = proj_in.shape
+    ways = lax.axis_size("row")
+    groups = features // GRP
+    quarters = ways // groups
+    pairs = GRP // 2 // quarters
+    bf16, f32 = jnp.bfloat16, jnp.float32
+
+    order = channel_order(groups, quarters, pairs)
+    hot_w = np.zeros((groups, GRP, GRP))
+    for g in range(groups):
+        hot_w[g, np.arange(GRP), order[g * GRP : (g + 1) * GRP] - g * GRP] = 1
+    w_out = jnp.einsum(
+        "gab,gbn->gan", jnp.asarray(hot_w, bf16), proj_out.reshape(groups, GRP, -1), preferred_element_type=f32
+    ).astype(bf16)
+    w_out = lax.all_gather(w_out.reshape(features, -1), "row", axis=1, tiled=True)
+
+    me = lax.axis_index("col")
+    other_w = lax.ppermute(proj_in, "col", [(0, 1), (1, 0)])
+    tok_spec = lambda pick: pl.BlockSpec((span, depth), pick)
+    whole = lambda shape: pl.BlockSpec(shape, lambda i, s: (0,) * len(shape))
+    part = pl.pallas_call(
+        own_kernel,
+        grid_spec=pltpu.PrefetchScalarGridSpec(
+            num_scalar_prefetch=1,
+            grid=(1,),
+            in_specs=[tok_spec(lambda i, s: (0, s[0])), whole((depth, features))],
+            out_specs=whole((span, features)),
+        ),
+        out_shape=jax.ShapeDtypeStruct((span, features), f32),
+        cost_estimate=pl.CostEstimate(flops=2 * span * depth * features, bytes_accessed=2 << 20, transcendentals=0),
+        name="own_half",
+    )(me[None], seq_rows, proj_in)
+    table = jnp.asarray(channel_table(quarters, pairs), bf16)
+    sent = pl.pallas_call(
+        send_kernel,
+        grid_spec=pltpu.PrefetchScalarGridSpec(
+            num_scalar_prefetch=1,
+            grid=(1,),
+            in_specs=[
+                tok_spec(lambda i, s: (0, s[0])),
+                whole((depth, features)),
+                whole((span, features)),
+                whole(table.shape),
+            ],
+            out_specs=whole((ways, 48, LANES)),
+            scratch_shapes=[pltpu.VMEM((2 * LANES, features), bf16)],
+        ),
+        out_shape=jax.ShapeDtypeStruct((ways, 48, LANES), bf16),
+        cost_estimate=pl.CostEstimate(flops=2 * span * depth * features, bytes_accessed=2 << 20, transcendentals=0),
+        name="send",
+    )((1 - me)[None], seq_rows, other_w, part, table)
+
+    held = lax.all_to_all(sent, "row", 0, 0, tiled=True)
+
+    even, odd = position_tables(ways, span)
+    even, odd = jnp.asarray(even, bf16), jnp.asarray(odd, bf16)
+    twist = jnp.asarray(twiddle_table(ways, span), f32)
+    special = lax.rem(lax.axis_index("row"), quarters)[None]
+    spectra = pl.pallas_call(
+        mix_kernel,
+        in_specs=[pl.BlockSpec(memory_space=pltpu.SMEM)] + vmem(4),
+        out_specs=vmem(1)[0],
+        out_shape=jax.ShapeDtypeStruct((ways, 48, LANES), bf16),
+        scratch_shapes=[pltpu.VMEM((ways * 32, 4 * LANES), bf16)],
+        name="mix",
+    )(special, held, even, odd, twist)
+
+    back = lax.all_to_all(spectra, "row", 0, 0, tiled=True)
+
+    hot = jnp.asarray(row_order(span), bf16)
+    result = pl.pallas_call(
+        out_kernel,
+        in_specs=vmem(3),
+        out_specs=vmem(1)[0],
+        out_shape=jax.ShapeDtypeStruct((span, w_out.shape[1]), bf16),
+        scratch_shapes=[pltpu.VMEM((span, features), bf16)],
+        name="out",
+    )(back, hot, w_out)
+    return result[None]
+
+
+def fits(mesh, tokens, proj_in, proj_out):
+    ways, cols = mesh.shape["row"], mesh.shape["col"]
+    features = proj_in.shape[1]
+    span = tokens.shape[1] // ways
+    return (
+        features % GRP == 0
+        and ways == 4 * (features // GRP) == 16
+        and span == 12 * ways
+        and cols == 2
+        and tokens.shape[0] == cols
+        and proj_out.shape[1] % (ways * LANES) == 0
+    )
+
+
 def solution(mesh):
     in_specs = (P("col", "row", None), P("col", None), P(None, "row"))
     out_specs = P("col", "row", None)
-    return jax.shard_map(shards, mesh=mesh, in_specs=in_specs, out_specs=out_specs, check_vma=False)
+
+    def run(tokens, proj_in, proj_out):
+        body = shards if fits(mesh, tokens, proj_in, proj_out) else general_shards
+        return jax.shard_map(body, mesh=mesh, in_specs=in_specs, out_specs=out_specs, check_vma=False)(
+            tokens, proj_in, proj_out
+        )
+
+    return run

time: 115 us -> 91 us (0.79)
  other arithmetic: 17.1 us -> 0 us
  Pallas kernels: 0 us -> 11.2 us
  matrix products: 10 us -> 1.73 us
  local copies, waits for them, and re-layouts: 7.43 us -> 2.56 us
  blocking collectives: 19.8 us -> 16.1 us
  waiting for transfers between devices: 40.3 us -> 36.7 us
  starting transfers between devices: 6.84 us -> 8.78 us
    unnamed x1 -> x0, other arithmetic: 17 us -> none
    all_to_all x1, waiting for transfers between devices: 24.7 us -> 8.94 us  [shards(): held = lax.all_to_all(sent, 'row', 0, 0, tiled=True)]
    all_gather x2 -> x1, waiting for transfers between devices: 14.2 us -> 27.8 us  [shards(): lax.all_gather(w_out.reshape(features, -1), 'row', axis=1, tiled=True)]
    pallas_call x0 -> x4, Pallas kernels: none -> 11.2 us  [the longest x1 3.53 us: shards(): pl.pallas_call(out_kernel, in_specs=vmem(3), out_specs=vmem(1)[0], out_sh...]
    dot_general x10 -> x1, matrix products: 10 us -> 1.73 us  [shards(): jnp.einsum('gab,gbn->gan', jnp.asarray(hot_w, bf16), proj_out.reshape(gro...]
    all_to_all x1, blocking collectives: 19.8 us -> 16.1 us  [shards(): back = lax.all_to_all(spectra, 'row', 0, 0, tiled=True)]
    all_to_all x3 -> x0, local copies, waits for them, and re-layouts: 1.75 us -> none  [shards(): lax.all_to_all(outgoing, 'row', split_axis=2, concat_axis=0, tiled=True)]
    another operation x3 -> x0, local copies, waits for them, and re-layouts: 1.65 us -> none  [the longest x1 1.09 us: shards(): jnp.stack([real_part.reshape(ways, per_dev, local_len), imag_part.reshape...]
  transfers between devices with their start and end apart: 3 -> 3, of which waited for: 2 -> 2; matrix products, arithmetic and copies ran while one was open for 27% -> 0% of each run, Pallas kernels for 0% -> 5%
where the time goes in v1:
time: 91 us; the launch traced here: 90.5 us
  waiting for transfers between devices  36.7 us (40%)
  blocking collectives  16.1 us (18%)
  between operations  13.4 us (15%)
  Pallas kernels  11.2 us (12%)
  starting transfers between devices  8.78 us (10%)
  local copies, waits for them, and re-layouts  2.56 us (3%)
  matrix products  1.73 us (2%)
    all_gather x1, waiting for transfers between devices, shards(): lax.all_gather(w_out.reshape(features, -1), 'row', axis=1, tiled=True)  27.8 us
    all_to_all x1, blocking collectives, shards(): back = lax.all_to_all(spectra, 'row', 0, 0, tiled=True)  16.1 us
    all_to_all x1, waiting for transfers between devices, shards(): held = lax.all_to_all(sent, 'row', 0, 0, tiled=True)  8.94 us
    all_to_all x1, starting transfers between devices, shards(): held = lax.all_to_all(sent, 'row', 0, 0, tiled=True)  8.22 us
    pallas_call x1, Pallas kernels, shards(): pl.pallas_call(out_kernel, in_specs=vmem(3), out_specs=vmem(1)[0], out_sh...  3.53 us
    pallas_call x1, Pallas kernels, shards(): pl.pallas_call(send_kernel, grid_spec=pltpu.PrefetchScalarGridSpec(num_sc...  2.79 us
    unnamed x6, local copies, waits for them, and re-layouts  2.56 us
    pallas_call x1, Pallas kernels, shards(): pl.pallas_call(own_kernel, grid_spec=pltpu.PrefetchScalarGridSpec(num_sca...  2.48 us
  transfers between devices with their start and end apart: 3, of which 2 were waited for; matrix products, arithmetic and copies ran while one was open for 0% of the time, Pallas kernels for 5%

profile of v1, /device:TPU:0, one launch (start us, length us, event | category | flops | bytes accessed | tf_op | source)
XLA Modules:
  0.0 90.5 jit_solution(14331960081516907033)
XLA Ops:
  6.5 0.0 copy-start
  6.5 0.0 all-gather.2.cloned.1.call-start
  6.5 0.9 copy-done
  7.4 1.7 %convolution_convert_fusion = bf16[4,128,128]{2,1,0:T(8,128)(2,1)} fusion(bf16[4,128,128]{2,1,0:T(8,128)(2,1)} %constant.27.clone, bf16[4,128,128]{2,1,0:T(8,128)(2,1)S(1)} %bitcast.9), kind=kOutput, calls=%fused_computation | convolution fusion | flops 16842752 | bytes 393216 | tf_op jit(solution)/shard_map/gab,gbn->gan/dot_general | solution.py:299
  9.2 0.0 all-gather.2.cloned.1.call-update
  9.2 0.6 collective-permute-start
  9.8 2.5 %own_half.1.part = f32[192,512]{1,0:T(8,128)} custom-call(s32[1]{0:T(128)} %bitcast.3.where, bf16[192,2048]{1,0:T(8,128)(2,1)} %bitcast.10, bf16[1024,512]{1,0:T(8,128)(2,1)} %w.1), custom_call_target="tpu_custom_call" | custom-call | flops 201326592 | bytes 2097152 | tf_op jit(solution)/shard_map/own_half/pallas_call | solution.py:308
  12.2 0.0 collective-permute-done.w
  12.2 0.0 copy-start.1
  12.3 1.0 %copy-done.1 = bf16[1024,512]{1,0:T(8,128)(2,1)} copy-done((bf16[1024,512]{1,0:T(8,128)(2,1)}, bf16[1024,512]{1,0:T(8,128)(2,1)S(1)}, u32[]{:S(2)}) %copy-start.1) | copy-done | bytes 1048600
  13.2 2.8 %send.1 = bf16[16,48,128]{2,1,0:T(8,128)(2,1)} custom-call(s32[1]{0:T(128)} %bitcast.1.where, bf16[192,2048]{1,0:T(8,128)(2,1)} %bitcast.11, bf16[1024,512]{1,0:T(8,128)(2,1)} %copy-done.1, f32[192,512]{1,0:T(8,128)} %own_half.1.part, bf16[128,128]{1,0:T(8,128)(2,1)} %constant.28.clone.table), custom_call_target="tpu_custom_call" | custom-call | flops 201326592 | bytes 2097152 | tf_op jit(solution)/shard_map/send/pallas_call | solution.py:321
  16.0 8.2 %all-to-all-start = ((bf16[16,48,128]{2,1,0:T(8,128)(2,1)}), bf16[16,48,128]{2,1,0:T(8,128)(2,1)S(1)}, u32[]{:S(2)}, u32[]{:S(2)}) async-start(bf16[16,48,128]{2,1,0:T(8,128)(2,1)} %send.1), calls=%async_computation | async-start | bytes 393216 | tf_op jit(solution)/shard_map/all_to_all | solution.py:340
  24.3 8.9 %all-to-all-done.x = bf16[16,48,128]{2,1,0:T(8,128)(2,1)S(1)} async-done(((bf16[16,48,128]{2,1,0:T(8,128)(2,1)}), bf16[16,48,128]{2,1,0:T(8,128)(2,1)S(1)}, u32[]{:S(2)}, u32[]{:S(2)}) %all-to-all-start) | async-done | bytes 196640 | tf_op jit(solution)/shard_map/all_to_all | solution.py:340
  33.2 0.0 copy-start.2
  33.2 0.7 copy-done.2
  33.9 2.4 %mix.1 = bf16[16,48,128]{2,1,0:T(8,128)(2,1)} custom-call(s32[1]{0:T(128)} %bitcast.special, bf16[16,48,128]{2,1,0:T(8,128)(2,1)} %copy-done.2, bf16[256,512]{1,0:T(8,128)(2,1)} %constant.29.clone.even, bf16[256,512]{1,0:T(8,128)(2,1)} %constant.30.clone.odd, f32[16,4,128]{2,1,0:T(4,128)} %constant.31.clone.twist), custom_call_target="tpu_custom_call" | custom-call | tf_op jit(solution)/shard_map/mix/pallas_call | solution.py:346
  36.3 16.1 %all_to_all.10.y = bf16[16,48,128]{2,1,0:T(8,128)(2,1)} all-to-all(bf16[16,48,128]{2,1,0:T(8,128)(2,1)} %mix.1), channel_id=1, replica_groups=mesh['row'=16,'col'=2] {'row'}, dimensions={0} | all-to-all | bytes 393216 | tf_op jit(solution)/shard_map/all_to_all | solution.py:355
  52.4 27.8 %all-gather.2.cloned.1.call-done.w = bf16[512,2048]{1,0:T(8,128)(2,1)} async-done(((bf16[512,128]{1,0:T(8,128)(2,1)}), bf16[512,2048]{1,0:T(8,128)(2,1)}) %all-gather.2.cloned.1.call-update) | async-done | bytes 2097168 | tf_op jit(solution)/shard_map/all_gather | solution.py:302
  80.2 3.5 %out.1 = bf16[192,2048]{1,0:T(8,128)(2,1)} custom-call(bf16[16,48,128]{2,1,0:T(8,128)(2,1)} %all_to_all.10.y, bf16[192,192]{1,0:T(8,128)(2,1)} %constant.32.clone.hot, bf16[512,2048]{1,0:T(8,128)(2,1)} %all-gather.2.cloned.1.call-done.w), custom_call_target="tpu_custom_call" | custom-call | tf_op jit(solution)/shard_map/out/pallas_call | solution.py:358
Async XLA Ops:
  6.5 0.9 copy-start
  6.5 73.6 %all-gather.2.cloned.1.call-start = ((), (), s32[]{:S(2)}) async-start(), calls=%async_computation.2 | async-start | bytes 2228224 | tf_op jit(solution)/shard_map/all_gather | solution.py:302
  9.2 3.1 %collective-permute-start = (bf16[1024,512]{1,0:T(8,128)(2,1)}, bf16[1024,512]{1,0:T(8,128)(2,1)S(1)}, u32[]{:S(2)}, u32[]{:S(2)}) collective-permute-start(bf16[1024,512]{1,0:T(8,128)(2,1)} %w.1), channel_id=1, source_target_pairs={{0,1},{1,0},{2,3},{3,2},{4,5},{5,4},{6,7},{7,6},{8,9},{9,8},{10,11... | collective-permute-start | bytes 3145736 | tf_op jit(solution)/shard_map/ppermute | solution.py:305
  12.2 1.0 %copy-start.1 = (bf16[1024,512]{1,0:T(8,128)(2,1)}, bf16[1024,512]{1,0:T(8,128)(2,1)S(1)}, u32[]{:S(2)}) copy-start(bf16[1024,512]{1,0:T(8,128)(2,1)S(1)} %collective-permute-done.w) | copy-start | bytes 3145732
  16.0 17.2 %all-to-all-start = ((bf16[16,48,128]{2,1,0:T(8,128)(2,1)}), bf16[16,48,128]{2,1,0:T(8,128)(2,1)S(1)}, u32[]{:S(2)}, u32[]{:S(2)}) async-start(bf16[16,48,128]{2,1,0:T(8,128)(2,1)} %send.1), calls=%async_computation | async-start | bytes 393216 | tf_op jit(solution)/shard_map/all_to_all | solution.py:340
  33.2 0.7 copy-start.2
Sparse Core Ops, SparseCore 0:
  10.0 70.0 all-gather.1
